TPU v7x, 32 devices: a whole 2x2x4 slice. The times are simulated.
32 devices in a mesh: sp: 8 (over z, x), tp: 4 (over y, core).
Axes of the slice: x: 2, y: 2, z: 4, core: 2. Of those that a mesh axis runs over, the one named last changes fastest.
Arguments:
- residual: bfloat16 [2048, 2048], P('sp', 'tp'), may hold values from -8 to 8
- query_latent: bfloat16 [2048, 512], P('sp'), may hold values from -6 to 6
- shared_latent: bfloat16 [2048, 256], P('sp'), may hold values from -6 to 6
- rotary_key: bfloat16 [2048, 32], P('sp'), may hold values from -300 to 300
- query_gain: float32 [512], replicated, may hold values from 0.1 to 1.9
- latent_gain: float32 [256], replicated, may hold values from 0.1 to 1.9
- query_narrow: bfloat16 [512, 384], P(None, 'tp'), may hold values from -0.5 to 0.5
- key_narrow: bfloat16 [256, 256], P(None, 'tp'), may hold values from -0.375 to 0.375
- value_narrow: bfloat16 [256, 256], P(None, 'tp'), may hold values from -0.375 to 0.375
- query_wide: bfloat16 [512, 640], P(None, 'tp'), may hold values from -0.5 to 0.5
- key_wide: bfloat16 [256, 512], P(None, 'tp'), may hold values from -0.375 to 0.375
- value_wide: bfloat16 [256, 512], P(None, 'tp'), may hold values from -0.375 to 0.375
- output_narrow: bfloat16 [256, 2048], P('tp'), may hold values from -1.75 to 1.75
- output_wide: bfloat16 [512, 2048], P('tp'), may hold values from -1.75 to 1.75
- first_gain: float32 [2048], P('tp'), may hold values from 0.1 to 1.9
- first_bias: float32 [2048], P('tp'), may hold values from -1.5 to 1.5
- gate_weight: bfloat16 [2048, 5632], P('sp', 'tp'), may hold values from -0.125 to 0.125
- up_weight: bfloat16 [2048, 5632], P('sp', 'tp'), may hold values from -0.125 to 0.125
- down_weight: bfloat16 [5632, 2048], P('tp', 'sp'), may hold values from -0.078125 to 0.078125
- second_gain: float32 [2048], P('tp'), may hold values from 0.1 to 1.9
- second_bias: float32 [2048], P('tp'), may hold values from -1.5 to 1.5
Outputs:
- layer_out: bfloat16 [2048, 2048], P('sp', 'tp')
All inputs are finite; a program needn't handle non-finite values.
Results may differ from a plain program's by a relative error of at most 0.017.
The roundings to bfloat16 on the way count: a program that leaves them out, or rounds other values in their place, can miss the bound.
Values may be sent and summed in bfloat16 or wider, within the bound.
A program may use at most 192 MiB of HBM per device.

v0:
```python
import functools

import jax
import jax.numpy as jnp
import numpy as np
from jax import lax
from jax.experimental import pallas as pl
from jax.experimental.pallas import tpu as pltpu
from jax.sharding import PartitionSpec as P

ROPE = 32
NOPE_A = 64
V_A = 64
NOPE_B = 128
V_B = 128
GRID_W = 64

EPS_ROOT = 1e-06
EPS_LAYER = 1e-05
THETA = 10000.0
DEEP_ALPHA = 2.0**0.25

KEY_BLOCK = 2048
ROW_TILE = 16
MESH = pl.DeviceIdType.MESH
BF = jnp.bfloat16
F32 = jnp.float32


def axial_tables(row_total):
    quarter = ROPE // 4
    freqs = np.float32(THETA) ** (-(2.0 * np.arange(quarter, dtype=np.float32)) / (2 * quarter))
    freqs = freqs.astype(np.float32)

    def spread(count, first):
        angle = np.arange(count, dtype=np.float32)[:, None] * freqs
        out = []
        for fn in (np.cos, np.sin):
            table = np.zeros((count, ROPE), np.float32)
            wave = fn(angle).astype(np.float32)
            start = 0 if first else ROPE // 2
            table[:, start : start + quarter] = wave
            table[:, start + quarter : start + 2 * quarter] = wave
            out.append(table)
        return out

    return spread(row_total // GRID_W, True) + spread(GRID_W, False)


def swap_matrix():
    quarter = ROPE // 4
    swap = np.zeros((ROPE, ROPE), np.float32)
    for base in (0, ROPE // 2):
        for i in range(quarter):
            swap[base + quarter + i, base + i] = -1.0
            swap[base + i, base + quarter + i] = 1.0
    return swap


def head_selectors(heads, plain):
    wide = plain + ROPE
    swap = swap_matrix()
    found = []
    for h in range(heads):
        keep = np.zeros((heads * wide, plain), np.float32)
        turn = np.zeros((heads * wide, ROPE), np.float32)
        flip = np.zeros((heads * wide, ROPE), np.float32)
        keep[h * wide : h * wide + plain] = np.eye(plain)
        turn[h * wide + plain : (h + 1) * wide] = np.eye(ROPE)
        flip[h * wide + plain : (h + 1) * wide] = swap
        found.append((keep, turn, flip))
    return [np.stack(group) for group in zip(*found)]


def split_groups(device_count, hidden_local, width, row_count):
    best = None
    for groups in range(1, device_count + 1):
        if device_count % groups or hidden_local % groups:
            continue
        moved = 3 * width * hidden_local // groups + 2 * row_count * groups * width
        if best is None or moved < best[0]:
            best = (moved, groups)
    return best[1]


def other(index, bit):
    return index + bit * (1 - 2 * ((index // bit) % 2))


def send(source, target, send_sem, recv_sem, sp, tp):
    return pltpu.make_async_remote_copy(
        src_ref=source,
        dst_ref=target,
        send_sem=send_sem,
        recv_sem=recv_sem,
        device_id={"sp": sp, "tp": tp},
        device_id_type=MESH,
    )


def dot(a, b):
    return jnp.dot(a, b, preferred_element_type=F32)


def across_dot(rows, columns):
    return lax.dot_general(
        rows, columns, (((1,), (1,)), ((), ())), preferred_element_type=F32
    )


def root_norm(values, gain):
    return values * lax.rsqrt(jnp.mean(values * values, axis=-1, keepdims=True) + EPS_ROOT) * gain


def layer_norm(values, gain, bias):
    center = jnp.mean(values, axis=-1, keepdims=True)
    moved = values - center
    spread = jnp.mean(moved * moved, axis=-1, keepdims=True)
    return moved * lax.rsqrt(spread + EPS_LAYER) * gain + bias


def layer_kernel(groups, turns, parts, *refs):
    (
        residual, query_latent, shared_latent, rotary_key, query_gain, latent_gain,
        query_narrow, key_narrow, value_narrow, query_wide, key_wide, value_wide,
        output_narrow, output_wide, first_gain, first_bias,
        gate_weight, up_weight, down_weight, second_gain, second_bias,
        row_cos, row_sin, col_cos, col_sin, swap, eye,
        keep_n, turn_n, flip_n, keep_w, turn_w, flip_w,
    ) = refs[:33]
    out_ref = refs[33]
    (
        raw, staged, weights, latents, cosine, sine, parts_f, raised, vals_n, vals_w,
        tops, totals, sums_n, sums_w, out_n, out_w, res_all, own_gains, gains,
        att_n, att_w, x_all, hidden, s1, r1, s2, r2, s3, r3, final,
    ) = refs[34:64]
    (
        load_sem, lzs, lzr, lxs, lxr, lcs, lcr, wzs, wzr, wxs, wxr, wls,
        tps, tpr, gns, gnr, ags, agr, ars, arr, p1s, p1r, p2s, p2r, p3s, p3r, fs, fr, fl,
    ) = refs[64:]
    sp, tp = lax.axis_index("sp"), lax.axis_index("tp")
    count = groups * turns
    group, turn = sp // turns, sp % turns
    low, high = tp % 2, tp // 2
    near, far = other(tp, 1), other(tp, 2)
    diag = other(far, 1)
    rows = query_latent.shape[0]
    width = x_all.shape[2]
    hidden_count, depth = weights.shape[2], weights.shape[3]
    quarter = rows // parts
    tail = []

    def group_at(k):
        return ((group + k) % groups) * turns + turn

    def turn_at(j):
        return group * turns + (turn + j) % turns

    def source_at(k, j):
        return ((group - k + groups) % groups) * turns + (turn - j + turns) % turns

    loads = []
    for i, (source, target) in enumerate(
        (
            (gate_weight, raw.at[0]),
            (up_weight, raw.at[1]),
            (down_weight, staged.at[2]),
            (output_narrow, out_n.at[tp]),
            (output_wide, out_w.at[tp]),
            (residual, res_all.at[tp]),
        )
    ):
        load = pltpu.make_async_copy(source, target, load_sem.at[i])
        load.start()
        loads.append(load)

    barrier = pltpu.get_barrier_semaphore()
    peers = [(group_at(k), tp) for k in range(1, groups)]
    peers += [(turn_at(j), tp) for j in range(1, turns)]
    peers += [(sp, near), (sp, far), (sp, diag)]
    for a, b in peers:
        pl.semaphore_signal(barrier, inc=1, device_id={"sp": a, "tp": b}, device_id_type=MESH)

    grid_rows = rows // GRID_W
    for i in range(grid_rows):
        at = pl.ds(i * GRID_W, GRID_W)
        line = pl.ds(sp * grid_rows + i, 1)
        cosine[at, :] = col_cos[...] + row_cos[line, :]
        sine[at, :] = col_sin[...] + row_sin[line, :]
    latents[sp, 0:rows, :] = root_norm(shared_latent[...].astype(F32), latent_gain[...]).astype(BF)
    rotary = rotary_key[...]
    turned = rotary.astype(F32) * cosine[...] + dot(rotary, swap[...]) * sine[...]
    latents[sp, rows : rows + ROPE, :] = across_dot(eye[...], turned.astype(BF)).astype(BF)
    for i, ref in enumerate((first_gain, first_bias, second_gain, second_bias)):
        own_gains[i : i + 1, :] = ref[...]
        gains[tp, i : i + 1, :] = ref[...]
    pl.semaphore_wait(barrier, len(peers))

    half = (rows + ROPE) // 2
    part = pl.ds(pl.multiple_of(low * half, half), half)
    lat_copies = []
    for k in range(1, groups):
        block = latents.at[sp, part]
        copy = send(block, block, lzs.at[k], lzr.at[k], group_at(k), tp)
        copy.start()
        lat_copies.append(copy)
    for j in range(1, turns):
        block = latents.at[sp, part]
        copy = send(block, block, lxs.at[0, j], lxr.at[0, j], turn_at(j), tp)
        copy.start()
        tail.append(copy.wait_send)

    def share(source, target, i):
        a = send(source, target.at[tp], tps.at[i, 0], tpr.at[i, 0], sp, far)
        b = send(source, target.at[tp], tps.at[i, 1], tpr.at[i, 1], sp, near)
        a.start()
        b.start()
        tail.append(a.wait_send)
        tail.append(b.wait_send)

        def onward():
            a.wait_recv()
            c = send(target.at[far], target.at[far], tps.at[i, 2], tpr.at[i, 2], sp, near)
            c.start()
            tail.append(c.wait_send)

            def done():
                b.wait_recv()
                c.wait_recv()

            return done

        return onward

    onward = [share(output_wide, out_w, 0), share(output_narrow, out_n, 1), share(residual, res_all, 2)]
    gain_copies = []
    for i, peer in enumerate((near, far, diag)):
        copy = send(own_gains, gains.at[tp], gns.at[i], gnr.at[i], sp, peer)
        copy.start()
        gain_copies.append(copy)
        tail.append(copy.wait_send)

    loads[0].wait()
    staged[0] = raw[0].T
    loads[1].wait()
    staged[1] = raw[1].T
    loads[2].wait()

    def piece(m, k):
        first = pl.multiple_of(((group + k) % groups) * hidden_count, 16)
        return staged.at[m, pl.ds(first, hidden_count)]

    weight_z = {}

    def send_weights(m):
        for k in range(1, groups):
            copy = send(piece(m, k), weights.at[m, sp], wzs.at[m, k], wzr.at[m, k], group_at(k), tp)
            copy.start()
            tail.append(copy.wait_send)
            weight_z[m, k] = copy
        local = pltpu.make_async_copy(piece(m, 0), weights.at[m, sp], wls.at[m])
        local.start()
        weight_z[m, 0] = local

    weight_x = {}

    def pass_weights(m, k):
        if k:
            weight_z[m, k].wait_recv()
        source = source_at(k, 0)
        block = weights.at[m, source] if k else piece(m, 0)
        for j in range(1, turns):
            copy = send(block, weights.at[m, source], wxs.at[m, k, j], wxr.at[m, k, j], turn_at(j), tp)
            copy.start()
            tail.append(copy.wait_send)
            weight_x[m, k, j] = copy

    def weights_here(m):
        weight_z[m, 0].wait()
        for k in range(groups):
            for j in range(1, turns):
                weight_x[m, k, j].wait_recv()

    send_weights(0)
    send_weights(1)

    shares = []

    def to_mate(k, j):
        block = latents.at[source_at(k, j), part]
        copy = send(block, block, lcs.at[k, j], lcr.at[k, j], sp, near)
        copy.start()
        tail.append(copy.wait_send)
        shares.append(copy)

    def latent_x(k, j):
        block = latents.at[sp, part]
        return send(block, block, lxs.at[k, j], lxr.at[k, j], turn_at(j), tp)

    for k in range(1, groups):
        lat_copies[k - 1].wait_recv()
        tail.append(lat_copies[k - 1].wait_send)
        block = latents.at[source_at(k, 0), part]
        for j in range(1, turns):
            copy = send(block, block, lxs.at[k, j], lxr.at[k, j], turn_at(j), tp)
            copy.start()
            tail.append(copy.wait_send)
        to_mate(k, 0)
    for m in range(2):
        pass_weights(m, 0)

    normed = root_norm(query_latent[...].astype(F32), query_gain[...]).astype(BF)
    scales = []
    heads = []
    for weight, keep, turns_m, flips, key_w, value_w, vals, sums, att, plain, value_dim in (
        (query_narrow, keep_n, turn_n, flip_n, key_narrow, value_narrow, vals_n, sums_n, att_n, NOPE_A, V_A),
        (query_wide, keep_w, turn_w, flip_w, key_wide, value_wide, vals_w, sums_w, att_w, NOPE_B, V_B),
    ):
        for h in range(keep.shape[0]):
            whole = weight[...]
            plain_q = dot(normed, dot(whole, keep[h]).astype(BF)).astype(BF)
            turn_q = dot(normed, dot(whole, turns_m[h]).astype(BF))
            flip_q = dot(normed, dot(whole, flips[h]).astype(BF))
            turn_q = (turn_q * cosine[...] + flip_q * sine[...]).astype(BF)
            heads.append((plain_q, turn_q, key_w, value_w, vals, sums, att, h, plain, value_dim))

    for k in range(groups):
        for j in range(1, turns):
            latent_x(k, j).wait_recv()
            to_mate(k, j)
    for copy in shares:
        copy.wait_recv()

    per = min(KEY_BLOCK // rows, count)
    blocks = count // per
    for n in range(len(heads)):
        tops[n] = jnp.full(tops.shape[1:], -jnp.inf, F32)
        totals[n] = jnp.zeros(totals.shape[1:], F32)
    sums_n[...] = jnp.zeros(sums_n.shape, F32)
    sums_w[...] = jnp.zeros(sums_w.shape, F32)

    def attend(b, carry):
        for n, (plain_q, turn_q, key_w, value_w, vals, sums, att, h, plain, value_dim) in enumerate(heads):
            for s in range(per):
                shard = b * per + s
                rows_here = latents[shard, 0:rows, :]
                keys = dot(rows_here, key_w[:, h * plain : (h + 1) * plain]).astype(BF)
                scores = across_dot(plain_q, keys) + dot(turn_q, latents[shard, rows : rows + ROPE, :])
                parts_f[n, :, s * rows : (s + 1) * rows] = scores
                vals[s * rows : (s + 1) * rows, :] = dot(
                    rows_here, value_w[:, h * value_dim : (h + 1) * value_dim]
                ).astype(BF)
            scale = (plain + ROPE) ** (-0.5)

            def tile(i, inner):
                at = pl.ds(pl.multiple_of(i * ROW_TILE, ROW_TILE), ROW_TILE)
                scores = parts_f[n, at, 0 : per * rows] * scale
                before = tops[n, at, :]
                largest = jnp.maximum(before[:, 0:1], jnp.max(scores, axis=-1, keepdims=True))
                lifted = jnp.exp(scores - largest)
                factor = jnp.exp(before - largest)
                tops[n, at, :] = jnp.broadcast_to(largest, before.shape)
                totals[n, at, :] = totals[n, at, :] * factor + jnp.sum(lifted, axis=-1, keepdims=True)
                raised[at, 0 : per * rows] = lifted.astype(BF)
                here = sums[h, at, :]
                sums[h, at, :] = here * factor[:, 0:1]
                return inner

            lax.fori_loop(0, rows // ROW_TILE, tile, 0)
            sums[h] = sums[h] + dot(raised[:, 0 : per * rows], vals[...])
        return carry

    if blocks == 1:
        attend(0, 0)
    else:
        lax.fori_loop(0, blocks, attend, 0)
    for n, (_, _, _, _, _, sums, att, h, _, value_dim) in enumerate(heads):
        att[tp, :, h * value_dim : (h + 1) * value_dim] = (sums[h] / totals[n][:, 0:1]).astype(BF)

    rest = [att_onward for att_onward in (share(att_w.at[tp], att_w, 3), share(att_n.at[tp], att_n, 4))]
    done = [step() for step in onward]
    for k in range(1, groups):
        pass_weights(0, k)
    done += [step() for step in rest]
    for step in done:
        step()
    for i in range(3, 6):
        loads[i].wait()
    for copy in gain_copies:
        copy.wait_recv()

    block_w = width // parts
    for c in range(parts):
        at = slice(c * block_w, (c + 1) * block_w)
        mixed = DEEP_ALPHA * res_all[c].astype(F32)
        for t in range(parts):
            mixed = mixed + dot(att_n[t], out_n[t, :, at])
            mixed = mixed + dot(att_w[t], out_w[t, :, at])
        parts_f[0, :, at] = mixed
    gain1 = jnp.concatenate([gains[t, 0:1, :] for t in range(parts)], axis=1)
    bias1 = jnp.concatenate([gains[t, 1:2, :] for t in range(parts)], axis=1)

    def first_norm(i, inner):
        at = pl.ds(pl.multiple_of(i * ROW_TILE, ROW_TILE), ROW_TILE)
        x_all[0, at, :] = layer_norm(parts_f[0, at, :], gain1, bias1).astype(BF)
        return inner

    lax.fori_loop(0, rows // ROW_TILE, first_norm, 0)

    def strip(t):
        return pl.ds(pl.multiple_of(t * quarter, quarter), quarter)

    ahead = [None]
    send_weights(2)
    pass_weights(2, 0)
    for k in range(1, groups):
        copy = send(
            x_all.at[0, strip(tp)], x_all.at[k, strip(tp)], ags.at[k], agr.at[k], group_at(k), tp
        )
        copy.start()
        tail.append(copy.wait_send)
        ahead.append(copy)
    for k in range(1, groups):
        pass_weights(1, k)
    for k in range(1, groups):
        pass_weights(2, k)

    relayed = {}

    def relay(k):
        ahead[k].wait_recv()
        block = x_all.at[k, strip(tp)]
        for i, peer in ((0, far), (1, near)):
            copy = send(block, block, ars.at[k, i], arr.at[k, i], sp, peer)
            copy.start()
            tail.append(copy.wait_send)
            relayed[k, i] = copy

    def relay_far(k):
        relayed[k, 0].wait_recv()
        block = x_all.at[k, strip(far)]
        copy = send(block, block, ars.at[k, 2], arr.at[k, 2], sp, near)
        copy.start()
        tail.append(copy.wait_send)
        relayed[k, 2] = copy

    firsts, seconds, thirds = [], [], [None]

    def compute(k):
        if k:
            relayed[k, 1].wait_recv()
            relayed[k, 2].wait_recv()
        if k == 0:
            weights_here(0)
            weights_here(1)
        gate = jnp.zeros((rows, hidden_count), F32)
        lifted = gate
        for i in range(count):
            columns = x_all[k, :, i * depth : (i + 1) * depth]
            gate += across_dot(columns, weights[0, i])
            lifted += across_dot(columns, weights[1, i])
        hidden[k] = (jax.nn.silu(gate) * lifted).astype(BF)

    def down(k):
        if k == 0:
            weights_here(2)
        for i in range(count):
            parts_f[k, :, i * depth : (i + 1) * depth] = dot(hidden[k], weights[2, i])
        for h in range(2):
            s1[k, h] = parts_f[k, strip(2 * h + 1 - low), :].astype(BF)
        firsts.append(send(s1.at[k], r1.at[k], p1s.at[k], p1r.at[k], sp, near))
        firsts[k].start()
        tail.append(firsts[k].wait_send)

    def second(k):
        firsts[k].wait_recv()
        kept = parts_f[k, strip(2 * (1 - high) + low), :]
        s2[k] = (kept + r1[k, 1 - high].astype(F32)).astype(BF)
        seconds.append(send(s2.at[k], r2.at[k], p2s.at[k], p2r.at[k], sp, far))
        seconds[k].start()
        tail.append(seconds[k].wait_send)

    def third(k):
        seconds[k].wait_recv()
        total = parts_f[k, strip(tp), :] + r1[k, high].astype(F32) + r2[k].astype(F32)
        if k == 0:
            parts_f[0, strip(tp), :] = total
        else:
            s3[k] = total.astype(BF)
            owner = source_at(k, 0)
            thirds.append(send(s3.at[k], r3.at[k], p3s.at[k], p3r.at[k], owner, tp))
            thirds[k].start()
            tail.append(thirds[k].wait_send)

    if groups > 1:
        relay(1)
    compute(0)
    if groups > 1:
        relay_far(1)
    for k in range(groups):
        if k + 2 < groups:
            relay(k + 2)
        down(k)
        if k + 1 < groups:
            compute(k + 1)
        if k + 2 < groups:
            relay_far(k + 2)
        second(k)
        if k >= 1:
            third(k - 1)
    third(groups - 1)

    for k in range(1, groups):
        thirds[k].wait_recv()
    gain2 = jnp.concatenate([gains[t, 2:3, :] for t in range(parts)], axis=1)
    bias2 = jnp.concatenate([gains[t, 3:4, :] for t in range(parts)], axis=1)
    for i in range(quarter // ROW_TILE):
        base = pl.multiple_of(tp * quarter + i * ROW_TILE, ROW_TILE)
        at = slice(i * ROW_TILE, (i + 1) * ROW_TILE)
        total = parts_f[0, pl.ds(base, ROW_TILE), :]
        for k in range(1, groups):
            total = total + r3[k, at, :].astype(F32)
        total = total + DEEP_ALPHA * x_all[0, pl.ds(base, ROW_TILE), :].astype(F32)
        result = layer_norm(total, gain2, bias2).astype(BF)
        for c in range(parts):
            final[c, at, :] = result[:, c * block_w : (c + 1) * block_w]
    finals = []
    for i, peer in enumerate((far, diag, near)):
        copy = send(final.at[peer], out_ref.at[strip(tp)], fs.at[i], fr.at[i], sp, peer)
        copy.start()
        finals.append(copy)
    local = pltpu.make_async_copy(final.at[tp], out_ref.at[strip(tp)], fl)
    local.start()
    for copy in finals:
        copy.wait_recv()
        copy.wait_send()
    local.wait()
    for wait in tail:
        wait()


def whole_layer(args, constants, groups, turns, parts):
    (
        residual, query_latent, shared_latent, rotary_key, query_gain, latent_gain,
        query_narrow, key_narrow, value_narrow, query_wide, key_wide, value_wide,
        output_narrow, output_wide, first_gain, first_bias,
        gate_weight, up_weight, down_weight, second_gain, second_bias,
    ) = args
    count = groups * turns
    rows, own_width = residual.shape
    width = own_width * parts
    depth, hidden_local = gate_weight.shape
    hidden_count = hidden_local // groups
    heads_n, heads_w = key_narrow.shape[1] // NOPE_A, key_wide.shape[1] // NOPE_B
    heads = heads_n + heads_w
    quarter = rows // parts
    keys = min(KEY_BLOCK, count * rows)
    latent_width = shared_latent.shape[1]
    dma = pltpu.SemaphoreType.DMA
    vm, far_ref = pl.BlockSpec(memory_space=pltpu.VMEM), pl.BlockSpec(memory_space=pl.ANY)
    names = [vm] * 21
    for i in (0, 12, 13, 16, 17, 18):
        names[i] = far_ref
    strip = (quarter, width)
    return pl.pallas_call(
        functools.partial(layer_kernel, groups, turns, parts),
        out_shape=jax.ShapeDtypeStruct(residual.shape, BF),
        in_specs=names + [vm] * len(constants),
        out_specs=vm,
        scratch_shapes=[
            pltpu.VMEM((2, depth, hidden_local), BF),
            pltpu.VMEM((3, hidden_local, depth), BF),
            pltpu.VMEM((3, count, hidden_count, depth), BF),
            pltpu.VMEM((count, rows + ROPE, latent_width), BF),
            pltpu.VMEM((rows, ROPE), F32),
            pltpu.VMEM((rows, ROPE), F32),
            pltpu.VMEM((max(groups, heads), rows, max(width, keys)), F32),
            pltpu.VMEM((rows, keys), BF),
            pltpu.VMEM((keys, V_A), BF),
            pltpu.VMEM((keys, V_B), BF),
            pltpu.VMEM((heads, rows, 128), F32),
            pltpu.VMEM((heads, rows, 128), F32),
            pltpu.VMEM((heads_n, rows, V_A), F32),
            pltpu.VMEM((heads_w, rows, V_B), F32),
            pltpu.VMEM((parts,) + output_narrow.shape, BF),
            pltpu.VMEM((parts,) + output_wide.shape, BF),
            pltpu.VMEM((parts,) + residual.shape, BF),
            pltpu.VMEM((8, own_width), F32),
            pltpu.VMEM((parts, 8, own_width), F32),
            pltpu.VMEM((parts, rows, heads_n * V_A), BF),
            pltpu.VMEM((parts, rows, heads_w * V_B), BF),
            pltpu.VMEM((groups, rows, width), BF),
            pltpu.VMEM((groups, rows, hidden_count), BF),
            pltpu.VMEM((groups, 2) + strip, BF),
            pltpu.VMEM((groups, 2) + strip, BF),
            pltpu.VMEM((groups,) + strip, BF),
            pltpu.VMEM((groups,) + strip, BF),
            pltpu.VMEM((groups,) + strip, BF),
            pltpu.VMEM((groups,) + strip, BF),
            pltpu.VMEM((parts, quarter, own_width), BF),
            dma((6,)),
            dma((groups,)),
            dma((groups,)),
            dma((groups, turns)),
            dma((groups, turns)),
            dma((groups, turns)),
            dma((groups, turns)),
            dma((3, groups)),
            dma((3, groups)),
            dma((3, groups, turns)),
            dma((3, groups, turns)),
            dma((3,)),
            dma((5, 3)),
            dma((5, 3)),
            dma((3,)),
            dma((3,)),
            dma((groups,)),
            dma((groups,)),
            dma((groups, 3)),
            dma((groups, 3)),
            dma((groups,)),
            dma((groups,)),
            dma((groups,)),
            dma((groups,)),
            dma((groups,)),
            dma((groups,)),
            dma((3,)),
            dma((3,)),
            dma(()),
        ],
        compiler_params=pltpu.CompilerParams(
            collective_id=0, has_side_effects=True, vmem_limit_bytes=62 * 2**20
        ),
        name="layer",
    )(*args, *constants)


def body(*args):
    args = [a.reshape(1, -1) if a.ndim == 1 else a for a in args]
    rows, own_width = args[0].shape
    device_count, parts = lax.axis_size("sp"), lax.axis_size("tp")
    hidden_local = args[16].shape[1]
    groups = split_groups(device_count, hidden_local, own_width * parts, rows)
    turns = device_count // groups
    constants = [jnp.asarray(t) for t in axial_tables(rows * device_count)]
    constants += [jnp.asarray(t, BF) for t in (swap_matrix(), np.eye(ROPE))]
    for weight, plain in ((args[6], NOPE_A), (args[9], NOPE_B)):
        heads = weight.shape[1] // (plain + ROPE)
        constants += [jnp.asarray(t, BF) for t in head_selectors(heads, plain)]
    return whole_layer(args, constants, groups, turns, parts)


def solution(mesh):
    return jax.shard_map(
        body,
        mesh=mesh,
        in_specs=(
            P("sp", "tp"),
            P("sp", None),
            P("sp", None),
            P("sp", None),
            P(),
            P(),
            P(None, "tp"),
            P(None, "tp"),
            P(None, "tp"),
            P(None, "tp"),
            P(None, "tp"),
            P(None, "tp"),
            P("tp", None),
            P("tp", None),
            P("tp"),
            P("tp"),
            P("sp", "tp"),
            P("sp", "tp"),
            P("tp", "sp"),
            P("tp"),
            P("tp"),
        ),
        out_specs=P("sp", "tp"),
        check_vma=False,
    )
```

profile of v0, /device:TPU:1, one launch (start us, length us, event | category | flops | bytes accessed | tf_op | source)
XLA Modules:
  0.0 152.9 jit_solution(7222321416006640740)
XLA Ops:
  0.0 0.0 copy-start.2
  0.0 0.0 copy-start.3
  0.0 1.4 copy.34.refs_3_
  1.4 0.0 copy-done.2
  1.5 0.0 copy-start.1
  1.5 0.7 copy.36.refs_7_
  2.2 0.0 copy-done.3
  2.2 0.0 copy-start
  2.2 0.7 copy.37.refs_8_
  2.9 0.0 copy-done.1
  2.9 0.8 copy.35.refs_6_
  3.7 0.0 copy-done
  3.7 0.8 copy.38.refs_9_
  4.5 146.7 %layer.1 = bf16[256,512]{1,0:T(8,128)(2,1)} custom-call(bf16[256,512]{1,0:T(8,128)(2,1)} %refs_0_.1, bf16[256,512]{1,0:T(8,128)(2,1)} %refs_1_.1, bf16[256,256]{1,0:T(8,128)(2,1)} %refs_2_.1, bf16[256,32]{1,0:T(8,128)(2,1)} %copy.34.refs_3_, f32[1,512]{1,0:T(1,128)} %bitcast.6, f32[1,256]{1,0:T(1,128)} %bitcast.11, bf16[512,96]{1,0:T(8,128)(2,1)} %copy.35.refs_6_, ...), custom_call_target="tpu_custom_call" | custom-call | tf_op jit(solution)/shard_map/layer/pallas_call | solution.py:565
  151.3 1.7 %copy.40 = bf16[256,512]{1,0:T(8,128)(2,1)} copy(bf16[256,512]{1,0:T(8,128)(2,1)} %layer.1) | data formatting | bytes 524288
Async XLA Ops:
  0.0 1.4 copy-start.2
  0.0 2.2 %copy-start.3 = (bf16[256,64]{0,1:T(8,128)(2,1)S(1)}, bf16[256,64]{0,1:T(8,128)(2,1)}, u32[]{:S(2)}) copy-start(bf16[256,64]{0,1:T(8,128)(2,1)} %param.41) | copy-start | bytes 98308
  1.5 1.5 copy-start.1
  2.2 1.5 copy-start
where the time goes:
time: 153 us
  Pallas kernels  147 us (96%)
  local copies, waits for them, and re-layouts  6.17 us (4%)
    pallas_call x1, Pallas kernels, whole_layer(): pl.pallas_call(functools.partial(layer_kernel, groups, turns, parts), out...  147 us
    unnamed x14, local copies, waits for them, and re-layouts  6.17 us

commit v1 on v0

v1 whole, which is shorter than its diff:
```python
import functools

import jax
import jax.numpy as jnp
import numpy as np
from jax import lax
from jax.experimental import pallas as pl
from jax.experimental.pallas import tpu as pltpu
from jax.sharding import PartitionSpec as P

ROPE = 32
NOPE_A = 64
V_A = 64
NOPE_B = 128
V_B = 128
GRID_W = 64

EPS_ROOT = 1e-06
EPS_LAYER = 1e-05
THETA = 10000.0
DEEP_ALPHA = 2.0**0.25

KEY_BLOCK = 2048
ROW_TILE = 16
MESH = pl.DeviceIdType.MESH
BF = jnp.bfloat16
F32 = jnp.float32


def axial_tables(row_total):
    quarter = ROPE // 4
    freqs = np.float32(THETA) ** (-(2.0 * np.arange(quarter, dtype=np.float32)) / (2 * quarter))
    freqs = freqs.astype(np.float32)

    def spread(count, first):
        angle = np.arange(count, dtype=np.float32)[:, None] * freqs
        out = []
        for fn in (np.cos, np.sin):
            table = np.zeros((count, ROPE), np.float32)
            wave = fn(angle).astype(np.float32)
            start = 0 if first else ROPE // 2
            table[:, start : start + quarter] = wave
            table[:, start + quarter : start + 2 * quarter] = wave
            out.append(table)
        return out

    return spread(row_total // GRID_W, True) + spread(GRID_W, False)


def swap_matrix():
    quarter = ROPE // 4
    swap = np.zeros((ROPE, ROPE), np.float32)
    for base in (0, ROPE // 2):
        for i in range(quarter):
            swap[base + i, base + quarter + i] = -1.0
            swap[base + quarter + i, base + i] = 1.0
    return swap


def split_groups(device_count, hidden_local, width, row_count):
    best = None
    for groups in range(1, device_count + 1):
        if device_count % groups or hidden_local % groups:
            continue
        moved = 3 * width * hidden_local // groups + 2 * row_count * groups * width
        if best is None or moved < best[0]:
            best = (moved, groups)
    return best[1]


def other(index, bit):
    return index + bit * (1 - 2 * ((index // bit) % 2))


def send(source, target, send_sem, recv_sem, sp, tp):
    return pltpu.make_async_remote_copy(
        src_ref=source,
        dst_ref=target,
        send_sem=send_sem,
        recv_sem=recv_sem,
        device_id={"sp": sp, "tp": tp},
        device_id_type=MESH,
    )


def dot(a, b):
    return jnp.dot(a, b, preferred_element_type=F32)


def across_dot(rows, columns):
    return lax.dot_general(
        rows, columns, (((1,), (1,)), ((), ())), preferred_element_type=F32
    )


def root_norm(values, gain):
    return values * lax.rsqrt(jnp.mean(values * values, axis=-1, keepdims=True) + EPS_ROOT) * gain


def layer_norm(values, gain, bias):
    center = jnp.mean(values, axis=-1, keepdims=True)
    moved = values - center
    spread = jnp.mean(moved * moved, axis=-1, keepdims=True)
    return moved * lax.rsqrt(spread + EPS_LAYER) * gain + bias


def chain_orders(groups):
    found = []
    for g in range(groups):
        found.append(sorted(range(groups), key=lambda s: (abs(s - g), s)))
    return found


def pick(index, options):
    value = options[-1]
    for i, option in enumerate(options[:-1]):
        value = jnp.where(index == i, option, value)
    return value


def layer_kernel(groups, turns, parts, *refs):
    (
        residual, query_latent, shared_latent, rotary_key, query_gain, latent_gain,
        query_narrow, key_narrow, value_narrow, query_wide, key_wide, value_wide,
        output_narrow, output_wide, first_gain, first_bias,
        gate_weight, up_weight, down_weight, second_gain, second_bias,
        row_cos, row_sin, col_cos, col_sin, swap,
    ) = refs[:26]
    out_ref = refs[26]
    (
        raw, staged, weights, latents, cosine, sine, board, parts_f, raised, key_all, value_all, vals,
        peaks, tops, totals, sums, out_n, out_w, res_all, own_gains, gains,
        att_n, att_w, x_all, hidden, s1, r1, s2, r2, s3, r3, final,
    ) = refs[27:59]
    (
        load_sem, lzs, lzr, lxs, lxr, lcs, lcr, wzs, wzr, wxs, wxr, wls,
        tps, tpr, gns, gnr, ags, agr, ars, arr, p1s, p1r, p2s, p2r, p3s, p3r, fs, fr, fl,
    ) = refs[59:]
    sp, tp = lax.axis_index("sp"), lax.axis_index("tp")
    count = groups * turns
    group, turn = sp // turns, sp % turns
    low, high = tp % 2, tp // 2
    near, far = other(tp, 1), other(tp, 2)
    diag = other(far, 1)
    rows = query_latent.shape[0]
    width = residual.shape[1] * parts
    hidden_count, depth = weights.shape[2], weights.shape[3]
    quarter = rows // parts
    orders = chain_orders(groups)
    sources = [group] + [pick(group, [orders[g][k] for g in range(groups)]) for k in range(1, groups)]
    heads_w, heads_n = key_wide.shape[1] // NOPE_B, key_narrow.shape[0] // NOPE_A
    tail = []

    def group_at(k):
        return ((group + k) % groups) * turns + turn

    def turn_at(j):
        return group * turns + (turn + j) % turns

    def source_at(k, j):
        return ((group - k + groups) % groups) * turns + (turn - j + turns) % turns

    wide_v, narrow_v = heads_w * V_B, heads_n * V_A
    own_w = pl.ds(pl.multiple_of(tp * wide_v, 16), wide_v)
    own_n = pl.ds(pl.multiple_of(tp * narrow_v, 16), narrow_v)
    loads = []
    for i, (source, target) in enumerate(
        (
            (gate_weight, raw.at[0]),
            (up_weight, raw.at[1]),
            (down_weight, staged.at[2]),
            (output_narrow, out_n.at[own_n]),
            (output_wide, out_w.at[own_w]),
            (residual, res_all.at[tp]),
        )
    ):
        load = pltpu.make_async_copy(source, target, load_sem.at[i])
        load.start()
        loads.append(load)

    barrier = pltpu.get_barrier_semaphore()
    peers = [(group_at(k), tp) for k in range(1, groups)]
    peers += [(turn_at(j), tp) for j in range(1, turns)]
    peers += [(sp, near), (sp, far), (sp, diag)]
    for a, b in peers:
        pl.semaphore_signal(barrier, inc=1, device_id={"sp": a, "tp": b}, device_id_type=MESH)

    grid_rows = rows // GRID_W
    for i in range(grid_rows):
        at = pl.ds(i * GRID_W, GRID_W)
        line = pl.ds(sp * grid_rows + i, 1)
        cosine[at, :] = col_cos[...] + row_cos[line, :]
        sine[at, :] = col_sin[...] + row_sin[line, :]
    latents[sp, 0:rows, :] = root_norm(shared_latent[...].astype(F32), latent_gain[...]).astype(BF)
    rotary = rotary_key[...]
    turned = rotary.astype(F32) * cosine[...].T + dot(swap[...], rotary) * sine[...].T
    latents[sp, rows : rows + ROPE, :] = turned.astype(BF)
    own_gains[...] = jnp.zeros(own_gains.shape, F32)
    for i, ref in enumerate((first_gain, first_bias, second_gain, second_bias)):
        own_gains[i : i + 1, :] = ref[...]
        gains[tp, i : i + 1, :] = ref[...]
    pl.semaphore_wait(barrier, len(peers))

    half = (rows + ROPE) // 2
    part = pl.ds(pl.multiple_of(low * half, half), half)
    lat_copies = []
    for k in range(1, groups):
        block = latents.at[sp, part]
        copy = send(block, block, lzs.at[k], lzr.at[k], group_at(k), tp)
        copy.start()
        lat_copies.append(copy)
    for j in range(1, turns):
        block = latents.at[sp, part]
        copy = send(block, block, lxs.at[0, j], lxr.at[0, j], turn_at(j), tp)
        copy.start()
        tail.append(copy.wait_send)

    def share(source, view, i):
        a = send(source, view(tp), tps.at[i, 0], tpr.at[i, 0], sp, far)
        b = send(source, view(tp), tps.at[i, 1], tpr.at[i, 1], sp, near)
        a.start()
        b.start()
        tail.append(a.wait_send)
        tail.append(b.wait_send)

        def onward():
            a.wait_recv()
            c = send(view(far), view(far), tps.at[i, 2], tpr.at[i, 2], sp, near)
            c.start()
            tail.append(c.wait_send)

            def done():
                b.wait_recv()
                c.wait_recv()

            return done

        return onward

    onward = [
        share(output_wide, lambda t: out_w.at[pl.ds(pl.multiple_of(t * wide_v, 16), wide_v)], 0),
        share(output_narrow, lambda t: out_n.at[pl.ds(pl.multiple_of(t * narrow_v, 16), narrow_v)], 1),
        share(residual, lambda t: res_all.at[t], 2),
    ]
    gain_copies = []
    for i, peer in enumerate((near, far, diag)):
        copy = send(own_gains, gains.at[tp], gns.at[i], gnr.at[i], sp, peer)
        copy.start()
        gain_copies.append(copy)
        tail.append(copy.wait_send)

    loads[0].wait()
    staged[0] = raw[0].T
    loads[1].wait()
    staged[1] = raw[1].T
    loads[2].wait()

    def piece(m, k):
        first = pl.multiple_of(((group + k) % groups) * hidden_count, 16)
        return staged.at[m, pl.ds(first, hidden_count)]

    weight_z = {}

    def send_weights(m):
        for k in range(1, groups):
            copy = send(piece(m, k), weights.at[m, sp], wzs.at[m, k], wzr.at[m, k], group_at(k), tp)
            copy.start()
            tail.append(copy.wait_send)
            weight_z[m, k] = copy
        local = pltpu.make_async_copy(piece(m, 0), weights.at[m, sp], wls.at[m])
        local.start()
        weight_z[m, 0] = local

    weight_x = {}

    def pass_weights(m, k):
        if k:
            weight_z[m, k].wait_recv()
        source = source_at(k, 0)
        block = weights.at[m, source] if k else piece(m, 0)
        for j in range(1, turns):
            copy = send(block, weights.at[m, source], wxs.at[m, k, j], wxr.at[m, k, j], turn_at(j), tp)
            copy.start()
            tail.append(copy.wait_send)
            weight_x[m, k, j] = copy

    def weights_here(m, k):
        if k == 0:
            weight_z[m, 0].wait()
        for j in range(1, turns):
            weight_x[m, k, j].wait_recv()

    send_weights(0)
    send_weights(1)

    normed = root_norm(query_latent[...].astype(F32), query_gain[...]).astype(BF)
    heads = []
    for weight, plain, value_dim, head_count, first_key, first_value in (
        (query_wide, NOPE_B, V_B, heads_w, 0, 0),
        (query_narrow, NOPE_A, V_A, heads_n, heads_w * NOPE_B, wide_v),
    ):
        for h in range(head_count):
            first = h * (plain + ROPE)
            turn_w = weight[first + plain : first + plain + ROPE, :]
            plain_q = across_dot(normed, weight[first : first + plain, :]).astype(BF)
            turn_q = across_dot(normed, turn_w)
            flip_q = across_dot(normed, dot(swap[...], turn_w).astype(BF))
            turn_q = (turn_q * cosine[...] + flip_q * sine[...]).astype(BF)
            query = jnp.concatenate([plain_q, turn_q], axis=1)
            heads.append((query, plain, value_dim, first_key + h * plain, first_value + h * value_dim))
    key_all[0 : heads_w * NOPE_B, :] = key_wide[...].T
    key_all[heads_w * NOPE_B :, :] = key_narrow[...]
    value_all[:, 0:wide_v] = value_wide[...]
    value_all[:, wide_v:] = value_narrow[...].T

    shares = {}

    def to_mate(k, j):
        block = latents.at[source_at(k, j), part]
        copy = send(block, block, lcs.at[k, j], lcr.at[k, j], sp, near)
        copy.start()
        tail.append(copy.wait_send)
        shares[k, j] = copy

    def latent_x(k, j):
        block = latents.at[sp, part]
        return send(block, block, lxs.at[k, j], lxr.at[k, j], turn_at(j), tp)

    for k in range(1, groups):
        lat_copies[k - 1].wait_recv()
        tail.append(lat_copies[k - 1].wait_send)
        block = latents.at[source_at(k, 0), part]
        for j in range(1, turns):
            copy = send(block, block, lxs.at[k, j], lxr.at[k, j], turn_at(j), tp)
            copy.start()
            tail.append(copy.wait_send)
        to_mate(k, 0)
    for m in range(2):
        pass_weights(m, 0)

    per = min(KEY_BLOCK // rows, count)
    blocks = count // per
    peaks[...] = jnp.full(peaks.shape, -jnp.inf, F32)
    tops[...] = jnp.full(tops.shape, -jnp.inf, F32)
    totals[...] = jnp.zeros(totals.shape, F32)
    sums[...] = jnp.zeros(sums.shape, F32)

    def score(shard, slot):
        rows_here = latents[shard, 0:rows, :]
        turned_here = latents[shard, rows : rows + ROPE, :]
        keys = across_dot(key_all[...], rows_here).astype(BF)
        vals[pl.ds(slot * rows, rows), :] = dot(rows_here, value_all[...]).astype(BF)
        for n, (query, plain, _, first_key, _) in enumerate(heads):
            joined = jnp.concatenate([keys[first_key : first_key + plain], turned_here], axis=0)
            scores = dot(query, joined)
            board[n, :, slot * rows : (slot + 1) * rows] = scores
            best = peaks[n]
            for c in range(0, rows, 128):
                best = jnp.maximum(best, scores[:, c : c + 128])
            peaks[n] = best

    def gather_softmax():
        for n, (_, plain, value_dim, _, first_value) in enumerate(heads):
            scale = (plain + ROPE) ** (-0.5) * 1.4426950408889634
            before = tops[n]
            largest = jnp.broadcast_to(jnp.max(peaks[n], axis=-1, keepdims=True), before.shape) * scale
            factor = jnp.exp2(before - largest)
            tops[n] = largest
            totals[n] = totals[n] * factor
            at_v = slice(first_value, first_value + value_dim)
            sums[:, at_v] = sums[:, at_v] * factor[:, 0:1]

            def tile(i, inner):
                at = pl.ds(pl.multiple_of(i * ROW_TILE, ROW_TILE), ROW_TILE)
                top = tops[n, at, :]
                total = totals[n, at, :]
                for c in range(0, per * rows, 128):
                    lifted = jnp.exp2(board[n, at, c : c + 128] * scale - top)
                    total = total + lifted
                    raised[at, c : c + 128] = lifted.astype(BF)
                totals[n, at, :] = total
                return inner

            lax.fori_loop(0, rows // ROW_TILE, tile, 0)
            sums[:, at_v] = sums[:, at_v] + dot(raised[...], vals[:, at_v])

    if blocks == 1:
        slot = 0
        score(sp, slot)
        for k in range(1, groups):
            shares[k, 0].wait_recv()
            slot += 1
            score(source_at(k, 0), slot)
        for k in range(groups):
            for j in range(1, turns):
                latent_x(k, j).wait_recv()
                to_mate(k, j)
        pass_weights(0, 1)
        for k in range(groups):
            for j in range(1, turns):
                shares[k, j].wait_recv()
                slot += 1
                score(source_at(k, j), slot)
        gather_softmax()
    else:
        for k in range(1, groups):
            shares[k, 0].wait_recv()
        for k in range(groups):
            for j in range(1, turns):
                latent_x(k, j).wait_recv()
                to_mate(k, j)
        pass_weights(0, 1)
        for k in range(groups):
            for j in range(1, turns):
                shares[k, j].wait_recv()

        def attend(b, carry):
            for s in range(per):
                score(b * per + s, s)
            gather_softmax()
            return carry

        lax.fori_loop(0, blocks, attend, 0)
    for n, (_, _, value_dim, _, first_value) in enumerate(heads):
        total = jnp.sum(totals[n], axis=-1, keepdims=True)
        result = (sums[:, first_value : first_value + value_dim] / total).astype(BF)
        if first_value < wide_v:
            for t in range(parts):
                place = t * wide_v + first_value

                @pl.when(tp == t)
                def _():
                    att_w[:, place : place + value_dim] = result
        else:
            place = first_value - wide_v
            att_n[tp, :, place : place + value_dim] = result

    rest = [
        share(
            att_w.at[:, pl.ds(pl.multiple_of(tp * wide_v, 128), wide_v)],
            lambda t: att_w.at[:, pl.ds(pl.multiple_of(t * wide_v, 128), wide_v)],
            3,
        ),
        share(att_n.at[tp], lambda t: att_n.at[t], 4),
    ]
    done = [step() for step in onward]
    for k in range(2, groups):
        pass_weights(0, k)
    done += [step() for step in rest]
    for step in done:
        step()
    for i in range(3, 6):
        loads[i].wait()
    for copy in gain_copies:
        copy.wait_recv()

    block_w = width // parts
    narrow = jnp.concatenate([att_n[t] for t in range(parts)], axis=1)
    run = jnp.zeros((rows, 128), F32)
    for c in range(parts):
        at = slice(c * block_w, (c + 1) * block_w)
        mixed = dot(att_w[...], out_w[:, at]) + dot(narrow, out_n[:, at])
        mixed = mixed + DEEP_ALPHA * res_all[c].astype(F32)
        board[0, :, at] = mixed
        for b in range(0, block_w, 128):
            run = run + mixed[:, b : b + 128]
    tops[0] = jnp.broadcast_to(jnp.sum(run, axis=-1, keepdims=True) / width, run.shape)

    def moments(i, inner):
        at = pl.ds(pl.multiple_of(i * ROW_TILE, ROW_TILE), ROW_TILE)
        center = tops[0, at, :]
        square = jnp.zeros(center.shape, F32)
        for c in range(0, width, 128):
            moved = board[0, at, c : c + 128] - center
            square = square + moved * moved
        totals[0, at, :] = square
        return inner

    lax.fori_loop(0, rows // ROW_TILE, moments, 0)
    spread = jnp.sum(totals[0], axis=-1, keepdims=True) / width
    totals[0] = jnp.broadcast_to(lax.rsqrt(spread + EPS_LAYER), totals.shape[1:])

    def first_norm(i, inner):
        at = pl.ds(pl.multiple_of(i * ROW_TILE, ROW_TILE), ROW_TILE)
        center, scale = tops[0, at, :], totals[0, at, :]
        for c in range(0, width, 128):
            t, b = c // block_w, c % block_w
            moved = (board[0, at, c : c + 128] - center) * scale
            moved = moved * gains[t, 0:1, b : b + 128] + gains[t, 1:2, b : b + 128]
            x_all[group, at, c : c + 128] = moved.astype(BF)
        return inner

    lax.fori_loop(0, rows // ROW_TILE, first_norm, 0)

    def strip(t):
        return pl.ds(pl.multiple_of(t * quarter, quarter), quarter)

    def ahead(source, step):
        block = x_all.at[source, strip(tp)]
        target = (group + step) * turns + turn
        return send(block, block, ags.at[source, (step + 1) // 2], agr.at[source], target, tp)

    def maybe(condition, act):
        @pl.when(condition)
        def _():
            act()

    for step in (1, -1):
        inside = (group + step >= 0) & (group + step < groups)
        maybe(inside, lambda step=step: ahead(group, step).start())
        tail.append(
            lambda inside=inside, step=step: maybe(inside, lambda: ahead(group, step).wait_send())
        )
    send_weights(2)
    pass_weights(2, 0)
    for k in range(1, groups):
        pass_weights(1, k)

    relayed = {}

    def relay(k):
        source = sources[k]
        ahead(source, 1).wait_recv()
        for step in (1, -1):
            from_behind = source < group if step == 1 else source > group
            inside = from_behind & (group + step >= 0) & (group + step < groups)
            maybe(inside, lambda step=step: ahead(source, step).start())
            tail.append(
                lambda inside=inside, step=step: maybe(
                    inside, lambda: ahead(source, step).wait_send()
                )
            )
        block = x_all.at[source, strip(tp)]
        for i, peer in ((0, far), (1, near)):
            copy = send(block, block, ars.at[k, i], arr.at[k, i], sp, peer)
            copy.start()
            tail.append(copy.wait_send)
            relayed[k, i] = copy

    def relay_far(k):
        relayed[k, 0].wait_recv()
        block = x_all.at[sources[k], strip(far)]
        copy = send(block, block, ars.at[k, 2], arr.at[k, 2], sp, near)
        copy.start()
        tail.append(copy.wait_send)
        relayed[k, 2] = copy

    def compute(k):
        if k:
            relayed[k, 1].wait_recv()
            relayed[k, 2].wait_recv()
        gate = jnp.zeros((rows, hidden_count), F32)
        lifted = gate
        for i in range(count):
            columns = x_all[sources[k], :, i * depth : (i + 1) * depth]
            gate += across_dot(columns, weights[0, i])
            lifted += across_dot(columns, weights[1, i])
        hidden[k] = (jax.nn.silu(gate) * lifted).astype(BF)

    span = turns * depth

    def column_group(c):
        return (group - c + groups) % groups

    firsts, seconds, thirds = {}, {}, {}

    def down(c, k):
        for j in range(turns):
            source = column_group(c) * turns + j
            product = dot(hidden[k], weights[2, source])
            parts_f[c, pl.ds(k * rows, rows), j * depth : (j + 1) * depth] = product
        for h in range(2):
            first = pl.multiple_of(k * rows + (2 * h + 1 - low) * quarter, quarter)
            s1[c, k, h] = parts_f[c, pl.ds(first, quarter), :].astype(BF)
        firsts[c, k] = send(s1.at[c, k], r1.at[c, k], p1s.at[c, k], p1r.at[c, k], sp, near)
        firsts[c, k].start()
        tail.append(firsts[c, k].wait_send)

    def second(c, k):
        firsts[c, k].wait_recv()
        first = pl.multiple_of(k * rows + (2 * (1 - high) + low) * quarter, quarter)
        kept = parts_f[c, pl.ds(first, quarter), :]
        s2[c, k] = (kept + r1[c, k, 1 - high].astype(F32)).astype(BF)
        seconds[c, k] = send(s2.at[c, k], r2.at[c, k], p2s.at[c, k], p2r.at[c, k], sp, far)
        seconds[c, k].start()
        tail.append(seconds[c, k].wait_send)

    def third(c, k):
        seconds[c, k].wait_recv()
        first = pl.multiple_of(k * rows + tp * quarter, quarter)
        total = parts_f[c, pl.ds(first, quarter), :]
        total = total + r1[c, k, high].astype(F32) + r2[c, k].astype(F32)
        if k == 0:
            parts_f[c, pl.ds(first, quarter), :] = total
        else:
            s3[c, k] = total.astype(BF)
            place = r3.at[column_group(c), group]
            copy = send(
                s3.at[c, k], place, p3s.at[c, k], p3r.at[column_group(c), group],
                sources[k] * turns + turn, tp,
            )
            copy.start()
            tail.append(copy.wait_send)

    for k in range(1, groups):
        relay(k)
        if k == 1:
            for m in range(2):
                for q in range(groups):
                    weights_here(m, q)
        compute(k - 1) if k == 1 else None
        relay_far(k)
        compute(k) if k < groups - 1 else None
    for k in range(1, groups):
        pass_weights(2, k)
    compute(groups - 1)

    units = [(c, k) for c in range(groups) for k in (list(range(1, groups)) + [0])]
    lag = groups
    for i in range(len(units) + 2 * lag):
        if i < len(units):
            c, k = units[i]
            if k == 1 or groups == 1:
                weights_here(2, c)
            down(c, k)
        if 0 <= i - lag < len(units):
            second(*units[i - lag])
        if 0 <= i - 2 * lag < len(units):
            third(*units[i - 2 * lag])

    def arrival(c, k):
        place = r3.at[column_group(c), sources[k]]
        return send(
            place, place, p3s.at[c, k], p3r.at[column_group(c), sources[k]], sp, near
        )

    for c in range(groups):
        for k in range(1, groups):
            arrival(c, k).wait_recv()
    gain2 = jnp.concatenate([gains[t, 2:3, :] for t in range(parts)], axis=1)
    bias2 = jnp.concatenate([gains[t, 3:4, :] for t in range(parts)], axis=1)
    for i in range(quarter // ROW_TILE):
        base = pl.multiple_of(tp * quarter + i * ROW_TILE, ROW_TILE)
        at = slice(i * ROW_TILE, (i + 1) * ROW_TILE)
        pieces = []
        for g in range(groups):
            total = parts_f[(group - g + groups) % groups, pl.ds(base, ROW_TILE), 0:span]
            for k in range(1, groups):
                total = total + r3[g, sources[k], at, :].astype(F32)
            pieces.append(total)
        total = jnp.concatenate(pieces, axis=1)
        total = total + DEEP_ALPHA * x_all[group, pl.ds(base, ROW_TILE), :].astype(F32)
        result = layer_norm(total, gain2, bias2).astype(BF)
        for c in range(parts):
            final[c, at, :] = result[:, c * block_w : (c + 1) * block_w]
    finals = []
    for i, peer in enumerate((far, diag, near)):
        copy = send(final.at[peer], out_ref.at[strip(tp)], fs.at[i], fr.at[i], sp, peer)
        copy.start()
        finals.append(copy)
    local = pltpu.make_async_copy(final.at[tp], out_ref.at[strip(tp)], fl)
    local.start()
    for copy in finals:
        copy.wait_recv()
        copy.wait_send()
    local.wait()
    for wait in tail:
        wait()


def whole_layer(args, constants, groups, turns, parts):
    (
        residual, query_latent, shared_latent, rotary_key, query_gain, latent_gain,
        query_narrow, key_narrow, value_narrow, query_wide, key_wide, value_wide,
        output_narrow, output_wide, first_gain, first_bias,
        gate_weight, up_weight, down_weight, second_gain, second_bias,
    ) = args
    count = groups * turns
    rows, own_width = residual.shape
    width = own_width * parts
    depth, hidden_local = gate_weight.shape
    hidden_count = hidden_local // groups
    heads_n, heads_w = key_narrow.shape[0] // NOPE_A, key_wide.shape[1] // NOPE_B
    heads = heads_n + heads_w
    quarter = rows // parts
    keys = min(KEY_BLOCK, count * rows)
    latent_width = shared_latent.shape[1]
    dma = pltpu.SemaphoreType.DMA
    vm, far_ref = pl.BlockSpec(memory_space=pltpu.VMEM), pl.BlockSpec(memory_space=pl.ANY)
    names = [vm] * 21
    for i in (0, 12, 13, 16, 17, 18):
        names[i] = far_ref
    strip = (quarter, turns * depth)
    return pl.pallas_call(
        functools.partial(layer_kernel, groups, turns, parts),
        out_shape=jax.ShapeDtypeStruct(residual.shape, BF),
        in_specs=names + [vm] * len(constants),
        out_specs=vm,
        scratch_shapes=[
            pltpu.VMEM((2, depth, hidden_local), BF),
            pltpu.VMEM((3, hidden_local, depth), BF),
            pltpu.VMEM((3, count, hidden_count, depth), BF),
            pltpu.VMEM((count, rows + ROPE, latent_width), BF),
            pltpu.VMEM((rows, ROPE), F32),
            pltpu.VMEM((rows, ROPE), F32),
            pltpu.VMEM((heads, rows, max(width, keys)), F32),
            pltpu.VMEM((groups, groups * rows, turns * depth), F32),
            pltpu.VMEM((rows, keys), BF),
            pltpu.VMEM((heads_w * NOPE_B + heads_n * NOPE_A, latent_width), BF),
            pltpu.VMEM((latent_width, heads_w * V_B + heads_n * V_A), BF),
            pltpu.VMEM((keys, heads_w * V_B + heads_n * V_A), BF),
            pltpu.VMEM((heads, rows, 128), F32),
            pltpu.VMEM((heads, rows, 128), F32),
            pltpu.VMEM((heads, rows, 128), F32),
            pltpu.VMEM((rows, heads_w * V_B + heads_n * V_A), F32),
            pltpu.VMEM((parts * heads_n * V_A, width), BF),
            pltpu.VMEM((parts * heads_w * V_B, width), BF),
            pltpu.VMEM((parts,) + residual.shape, BF),
            pltpu.VMEM((8, own_width), F32),
            pltpu.VMEM((parts, 8, own_width), F32),
            pltpu.VMEM((parts, rows, heads_n * V_A), BF),
            pltpu.VMEM((rows, parts * heads_w * V_B), BF),
            pltpu.VMEM((groups, rows, width), BF),
            pltpu.VMEM((groups, rows, hidden_count), BF),
            pltpu.VMEM((groups, groups, 2) + strip, BF),
            pltpu.VMEM((groups, groups, 2) + strip, BF),
            pltpu.VMEM((groups, groups) + strip, BF),
            pltpu.VMEM((groups, groups) + strip, BF),
            pltpu.VMEM((groups, groups) + strip, BF),
            pltpu.VMEM((groups, groups) + strip, BF),
            pltpu.VMEM((parts, quarter, own_width), BF),
            dma((6,)),
            dma((groups,)),
            dma((groups,)),
            dma((groups, turns)),
            dma((groups, turns)),
            dma((groups, turns)),
            dma((groups, turns)),
            dma((3, groups)),
            dma((3, groups)),
            dma((3, groups, turns)),
            dma((3, groups, turns)),
            dma((3,)),
            dma((5, 3)),
            dma((5, 3)),
            dma((3,)),
            dma((3,)),
            dma((groups, 2)),
            dma((groups,)),
            dma((groups, 3)),
            dma((groups, 3)),
            dma((groups, groups)),
            dma((groups, groups)),
            dma((groups, groups)),
            dma((groups, groups)),
            dma((groups, groups)),
            dma((groups, groups)),
            dma((3,)),
            dma((3,)),
            dma(()),
        ],
        compiler_params=pltpu.CompilerParams(
            collective_id=0, has_side_effects=True, vmem_limit_bytes=62 * 2**20
        ),
        name="layer",
    )(*args, *constants)


def body(*args):
    args = [a.reshape(1, -1) if a.ndim == 1 else a for a in args]
    for i in (3, 6, 7, 8, 9):
        args[i] = args[i].T
    rows, own_width = args[0].shape
    device_count, parts = lax.axis_size("sp"), lax.axis_size("tp")
    hidden_local = args[16].shape[1]
    groups = split_groups(device_count, hidden_local, own_width * parts, rows)
    turns = device_count // groups
    constants = [jnp.asarray(t) for t in axial_tables(rows * device_count)]
    constants.append(jnp.asarray(swap_matrix(), BF))
    return whole_layer(args, constants, groups, turns, parts)


def solution(mesh):
    return jax.shard_map(
        body,
        mesh=mesh,
        in_specs=(
            P("sp", "tp"),
            P("sp", None),
            P("sp", None),
            P("sp", None),
            P(),
            P(),
            P(None, "tp"),
            P(None, "tp"),
            P(None, "tp"),
            P(None, "tp"),
            P(None, "tp"),
            P(None, "tp"),
            P("tp", None),
            P("tp", None),
            P("tp"),
            P("tp"),
            P("sp", "tp"),
            P("sp", "tp"),
            P("tp", "sp"),
            P("tp"),
            P("tp"),
        ),
        out_specs=P("sp", "tp"),
        check_vma=False,
    )
```

time: 153 us -> 133 us (0.87)
  Pallas kernels: 147 us -> 131 us
  local copies, waits for them, and re-layouts: 6.17 us -> 1.67 us
    pallas_call x1, Pallas kernels: 147 us -> 131 us  [whole_layer(): pl.pallas_call(functools.partial(layer_kernel, groups, turns, parts), out...]
    unnamed x14 -> x1, local copies, waits for them, and re-layouts: 6.17 us -> 1.67 us
where the time goes in v1:
time: 133 us; the launch traced here: 132 us
  Pallas kernels  131 us (98%)
  local copies, waits for them, and re-layouts  1.67 us (1%)
    pallas_call x1, Pallas kernels, whole_layer(): pl.pallas_call(functools.partial(layer_kernel, groups, turns, parts), out...  131 us

profile of v1, /device:TPU:1, one launch (start us, length us, event | category | flops | bytes accessed | tf_op | source)
XLA Modules:
  0.0 132.4 jit_solution(15792657866987303204)
XLA Ops:
  0.0 130.7 %layer.1 = bf16[256,512]{1,0:T(8,128)(2,1)} custom-call(bf16[256,512]{1,0:T(8,128)(2,1)} %refs_0_.1, bf16[256,512]{1,0:T(8,128)(2,1)} %refs_1_.1, bf16[256,256]{1,0:T(8,128)(2,1)} %refs_2_.1, bf16[32,256]{1,0:T(8,128)(2,1)} %bitcast.15, f32[1,512]{1,0:T(1,128)} %bitcast.16, f32[1,256]{1,0:T(1,128)} %bitcast.21, bf16[96,512]{1,0:T(8,128)(2,1)} %bitcast.12, ...), custom_call_target="tpu_custom_call" | custom-call | tf_op jit(solution)/shard_map/layer/pallas_call | solution.py:694
  130.7 1.7 %copy.28 = bf16[256,512]{1,0:T(8,128)(2,1)} copy(bf16[256,512]{1,0:T(8,128)(2,1)} %layer.1) | data formatting | bytes 524288

commit v2 on v1

--- a/solution.py
+++ b/solution.py
@@ -22,6 +22,7 @@
 
 KEY_BLOCK = 2048
 ROW_TILE = 16
+HELD = 3
 MESH = pl.DeviceIdType.MESH
 BF = jnp.bfloat16
 F32 = jnp.float32
@@ -107,7 +108,8 @@
 def chain_orders(groups):
     found = []
     for g in range(groups):
-        found.append(sorted(range(groups), key=lambda s: (abs(s - g), s)))
+        outward = 1 if 2 * g >= groups else -1
+        found.append(sorted(range(groups), key=lambda s: (abs(s - g), (g - s) * outward)))
     return found
 
 
@@ -118,14 +120,22 @@
     return value
 
 
-def layer_kernel(groups, turns, parts, *refs):
+def layer_kernel(groups, turns, parts, staged_inputs, *refs):
+    inputs, held, fetch_sem = refs[:26], refs[-1 - len(staged_inputs) : -1], refs[-1]
+    fetches = []
+    for i, place in enumerate(staged_inputs):
+        fetch = pltpu.make_async_copy(inputs[place], held[i], fetch_sem.at[i])
+        fetch.start()
+        fetches.append(fetch)
+        inputs = inputs[:place] + (held[i],) + inputs[place + 1 :]
+    refs = refs[: -1 - len(staged_inputs)]
     (
         residual, query_latent, shared_latent, rotary_key, query_gain, latent_gain,
         query_narrow, key_narrow, value_narrow, query_wide, key_wide, value_wide,
         output_narrow, output_wide, first_gain, first_bias,
         gate_weight, up_weight, down_weight, second_gain, second_bias,
         row_cos, row_sin, col_cos, col_sin, swap,
-    ) = refs[:26]
+    ) = inputs
     out_ref = refs[26]
     (
         raw, staged, weights, latents, cosine, sine, board, parts_f, raised, key_all, value_all, vals,
@@ -185,6 +195,9 @@
     for a, b in peers:
         pl.semaphore_signal(barrier, inc=1, device_id={"sp": a, "tp": b}, device_id_type=MESH)
 
+    for fetch in fetches:
+        fetch.wait()
+
     grid_rows = rows // GRID_W
     for i in range(grid_rows):
         at = pl.ds(i * GRID_W, GRID_W)
@@ -256,28 +269,32 @@
     loads[2].wait()
 
     def piece(m, k):
-        first = pl.multiple_of(((group + k) % groups) * hidden_count, 16)
+        first = pl.multiple_of(sources[k] * hidden_count, 16)
         return staged.at[m, pl.ds(first, hidden_count)]
 
     weight_z = {}
 
-    def send_weights(m):
-        for k in range(1, groups):
-            copy = send(piece(m, k), weights.at[m, sp], wzs.at[m, k], wzr.at[m, k], group_at(k), tp)
-            copy.start()
-            tail.append(copy.wait_send)
-            weight_z[m, k] = copy
+    def keep_weights(m):
         local = pltpu.make_async_copy(piece(m, 0), weights.at[m, sp], wls.at[m])
         local.start()
         weight_z[m, 0] = local
 
+    def send_weights(m, started):
+        for k in range(1, groups):
+            target = sources[k] * turns + turn
+            copy = send(piece(m, k), weights.at[m, sp], wzs.at[m, k], wzr.at[m, group], target, tp)
+            if k <= started:
+                copy.start()
+            tail.append(copy.wait_send)
+            weight_z[m, k] = copy
+
     weight_x = {}
 
     def pass_weights(m, k):
+        source = sources[k] * turns + turn
+        block = weights.at[m, source] if k else piece(m, 0)
         if k:
-            weight_z[m, k].wait_recv()
-        source = source_at(k, 0)
-        block = weights.at[m, source] if k else piece(m, 0)
+            send(block, block, wzs.at[m, k], wzr.at[m, sources[k]], sp, near).wait_recv()
         for j in range(1, turns):
             copy = send(block, weights.at[m, source], wxs.at[m, k, j], wxr.at[m, k, j], turn_at(j), tp)
             copy.start()
@@ -290,8 +307,10 @@
         for j in range(1, turns):
             weight_x[m, k, j].wait_recv()
 
-    send_weights(0)
-    send_weights(1)
+    send_weights(0, groups)
+    send_weights(1, HELD)
+    for m in range(3):
+        keep_weights(m)
 
     normed = root_norm(query_latent[...].astype(F32), query_gain[...]).astype(BF)
     heads = []
@@ -335,7 +354,7 @@
             copy.start()
             tail.append(copy.wait_send)
         to_mate(k, 0)
-    for m in range(2):
+    for m in range(3):
         pass_weights(m, 0)
 
     per = min(KEY_BLOCK // rows, count)
@@ -444,8 +463,6 @@
         share(att_n.at[tp], lambda t: att_n.at[t], 4),
     ]
     done = [step() for step in onward]
-    for k in range(2, groups):
-        pass_weights(0, k)
     done += [step() for step in rest]
     for step in done:
         step()
@@ -511,31 +528,50 @@
         tail.append(
             lambda inside=inside, step=step: maybe(inside, lambda: ahead(group, step).wait_send())
         )
-    send_weights(2)
-    pass_weights(2, 0)
-    for k in range(1, groups):
+    for k in range(HELD + 1, groups):
+        weight_z[1, k].start()
+    send_weights(2, 0)
+
+    def start_down(first=1, past=groups):
+        for k in range(first, past):
+            weight_z[2, k].start()
+
+    start_down(1, 2)
+    for k in range(2, groups):
+        pass_weights(0, k)
+    for k in range(1, groups - 1):
         pass_weights(1, k)
 
     relayed = {}
-
-    def relay(k):
+    edge = (group == 0) | (group == groups - 1)
+
+    def relay(k, only=None):
         source = sources[k]
-        ahead(source, 1).wait_recv()
+        block = x_all.at[source, strip(tp)]
+        steps = []
         for step in (1, -1):
             from_behind = source < group if step == 1 else source > group
             inside = from_behind & (group + step >= 0) & (group + step < groups)
-            maybe(inside, lambda step=step: ahead(source, step).start())
-            tail.append(
-                lambda inside=inside, step=step: maybe(
-                    inside, lambda: ahead(source, step).wait_send()
-                )
-            )
-        block = x_all.at[source, strip(tp)]
-        for i, peer in ((0, far), (1, near)):
-            copy = send(block, block, ars.at[k, i], arr.at[k, i], sp, peer)
-            copy.start()
-            tail.append(copy.wait_send)
-            relayed[k, i] = copy
+            steps.append((inside, ahead(source, step)))
+        if (k, 0) not in relayed:
+            for i, peer in ((0, far), (1, near)):
+                copy = send(block, block, ars.at[k, i], arr.at[k, i], sp, peer)
+                tail.append(copy.wait_send)
+                relayed[k, i] = copy
+            for inside, copy in steps:
+                tail.append(lambda inside=inside, copy=copy: maybe(inside, copy.wait_send))
+
+        def act():
+            steps[0][1].wait_recv()
+            for inside, copy in steps:
+                maybe(inside, copy.start)
+            for i in range(2):
+                relayed[k, i].start()
+
+        if only is None:
+            act()
+        else:
+            maybe(only, act)
 
     def relay_far(k):
         relayed[k, 0].wait_recv()
@@ -560,7 +596,7 @@
     span = turns * depth
 
     def column_group(c):
-        return (group - c + groups) % groups
+        return sources[c]
 
     firsts, seconds, thirds = {}, {}, {}
 
@@ -568,10 +604,10 @@
         for j in range(turns):
             source = column_group(c) * turns + j
             product = dot(hidden[k], weights[2, source])
-            parts_f[c, pl.ds(k * rows, rows), j * depth : (j + 1) * depth] = product
+            parts_f[column_group(c), pl.ds(k * rows, rows), j * depth : (j + 1) * depth] = product
         for h in range(2):
             first = pl.multiple_of(k * rows + (2 * h + 1 - low) * quarter, quarter)
-            s1[c, k, h] = parts_f[c, pl.ds(first, quarter), :].astype(BF)
+            s1[c, k, h] = parts_f[column_group(c), pl.ds(first, quarter), :].astype(BF)
         firsts[c, k] = send(s1.at[c, k], r1.at[c, k], p1s.at[c, k], p1r.at[c, k], sp, near)
         firsts[c, k].start()
         tail.append(firsts[c, k].wait_send)
@@ -579,7 +615,7 @@
     def second(c, k):
         firsts[c, k].wait_recv()
         first = pl.multiple_of(k * rows + (2 * (1 - high) + low) * quarter, quarter)
-        kept = parts_f[c, pl.ds(first, quarter), :]
+        kept = parts_f[column_group(c), pl.ds(first, quarter), :]
         s2[c, k] = (kept + r1[c, k, 1 - high].astype(F32)).astype(BF)
         seconds[c, k] = send(s2.at[c, k], r2.at[c, k], p2s.at[c, k], p2r.at[c, k], sp, far)
         seconds[c, k].start()
@@ -588,10 +624,10 @@
     def third(c, k):
         seconds[c, k].wait_recv()
         first = pl.multiple_of(k * rows + tp * quarter, quarter)
-        total = parts_f[c, pl.ds(first, quarter), :]
+        total = parts_f[column_group(c), pl.ds(first, quarter), :]
         total = total + r1[c, k, high].astype(F32) + r2[c, k].astype(F32)
         if k == 0:
-            parts_f[c, pl.ds(first, quarter), :] = total
+            parts_f[column_group(c), pl.ds(first, quarter), :] = total
         else:
             s3[c, k] = total.astype(BF)
             place = r3.at[column_group(c), group]
@@ -602,31 +638,79 @@
             copy.start()
             tail.append(copy.wait_send)
 
-    for k in range(1, groups):
+    waiting, moving = [], []
+
+    def push_second(left):
+        while len(waiting) > left:
+            second(*waiting[0])
+            moving.append(waiting.pop(0))
+
+    def push_third(left):
+        while len(moving) > left:
+            third(*moving.pop(0))
+
+    def unit(c, k):
+        down(c, k)
+        waiting.append((c, k))
+        push_second(2)
+        push_third(6)
+
+    last = groups - 1
+    for k in range(1, last):
         relay(k)
         if k == 1:
-            for m in range(2):
-                for q in range(groups):
-                    weights_here(m, q)
-        compute(k - 1) if k == 1 else None
-        relay_far(k)
-        compute(k) if k < groups - 1 else None
-    for k in range(1, groups):
-        pass_weights(2, k)
-    compute(groups - 1)
-
-    units = [(c, k) for c in range(groups) for k in (list(range(1, groups)) + [0])]
-    lag = groups
-    for i in range(len(units) + 2 * lag):
-        if i < len(units):
-            c, k = units[i]
-            if k == 1 or groups == 1:
-                weights_here(2, c)
-            down(c, k)
-        if 0 <= i - lag < len(units):
-            second(*units[i - lag])
-        if 0 <= i - 2 * lag < len(units):
-            third(*units[i - 2 * lag])
+            pass_weights(1, last)
+    maybe(edge, lambda: start_down(2, max(last, 2)))
+    if last > 1:
+        relay_far(1)
+    if last > 0:
+        relay(last, ~edge)
+    maybe(~edge, lambda: start_down(2, max(last, 2)))
+    if last == 1:
+        pass_weights(1, last)
+    if last > 0:
+        pass_weights(2, 1)
+    for m in range(2):
+        for q in range(groups):
+            weights_here(m, q)
+    compute(0)
+    if last > 1:
+        compute(1)
+    start_down(max(last, 2))
+    weights_here(2, 0)
+    early = [*range(1, last), 0]
+    for k in early[:1] + early[-1:] + early[1:-1] if last > 1 else [0]:
+        if k > 1:
+            relay_far(k)
+            compute(k)
+        unit(0, k)
+    push_second(0)
+    if last > 0:
+        relay(last, edge)
+        weights_here(2, 1)
+        for k in early:
+            unit(1, k)
+        push_second(0)
+        for c in range(2, groups):
+            pass_weights(2, c)
+        push_third(3)
+        relay_far(last)
+    for c in range(2, groups):
+        weights_here(2, c)
+        if c > 2:
+            unit(c, last)
+        for k in early:
+            unit(c, k)
+        if c == 2:
+            compute(last)
+            for b in range(3):
+                unit(b, last)
+    if last in (1, 2):
+        compute(last)
+        for c in range(groups):
+            unit(c, last)
+    push_second(0)
+    push_third(0)
 
     def arrival(c, k):
         place = r3.at[column_group(c), sources[k]]
@@ -644,7 +728,7 @@
         at = slice(i * ROW_TILE, (i + 1) * ROW_TILE)
         pieces = []
         for g in range(groups):
-            total = parts_f[(group - g + groups) % groups, pl.ds(base, ROW_TILE), 0:span]
+            total = parts_f[g, pl.ds(base, ROW_TILE), :]
             for k in range(1, groups):
                 total = total + r3[g, sources[k], at, :].astype(F32)
             pieces.append(total)
@@ -686,16 +770,15 @@
     keys = min(KEY_BLOCK, count * rows)
     latent_width = shared_latent.shape[1]
     dma = pltpu.SemaphoreType.DMA
-    vm, far_ref = pl.BlockSpec(memory_space=pltpu.VMEM), pl.BlockSpec(memory_space=pl.ANY)
-    names = [vm] * 21
-    for i in (0, 12, 13, 16, 17, 18):
-        names[i] = far_ref
+    far_ref = pl.BlockSpec(memory_space=pl.ANY)
+    operands = [*args, *constants]
+    staged_inputs = [i for i in range(len(operands)) if i not in (0, 12, 13, 16, 17, 18)]
     strip = (quarter, turns * depth)
     return pl.pallas_call(
-        functools.partial(layer_kernel, groups, turns, parts),
+        functools.partial(layer_kernel, groups, turns, parts, staged_inputs),
         out_shape=jax.ShapeDtypeStruct(residual.shape, BF),
-        in_specs=names + [vm] * len(constants),
-        out_specs=vm,
+        in_specs=[far_ref] * len(operands),
+        out_specs=far_ref,
         scratch_shapes=[
             pltpu.VMEM((2, depth, hidden_local), BF),
             pltpu.VMEM((3, hidden_local, depth), BF),
@@ -758,12 +841,14 @@
             dma((3,)),
             dma((3,)),
             dma(()),
+            *[pltpu.VMEM(operands[i].shape, operands[i].dtype) for i in staged_inputs],
+            dma((len(staged_inputs),)),
         ],
         compiler_params=pltpu.CompilerParams(
             collective_id=0, has_side_effects=True, vmem_limit_bytes=62 * 2**20
         ),
         name="layer",
-    )(*args, *constants)
+    )(*operands)
 
 
 def body(*args):

time: 133 us -> 111 us (0.83)
  Pallas kernels: 131 us -> 110 us
    pallas_call x1, Pallas kernels: 131 us -> 110 us  [whole_layer(): pl.pallas_call(functools.partial(layer_kernel, groups, turns, parts, stag...]
where the time goes in v2:
time: 111 us
  Pallas kernels  110 us (99%)
  local copies, waits for them, and re-layouts  1.67 us (2%)
    pallas_call x1, Pallas kernels, whole_layer(): pl.pallas_call(functools.partial(layer_kernel, groups, turns, parts, stag...  110 us

profile of v2, /device:TPU:1, one launch (start us, length us, event | category | flops | bytes accessed | tf_op | source)
XLA Modules:
  0.0 111.2 jit_solution(7826046016960251880)
XLA Ops:
  0.0 109.5 %layer.1 = bf16[256,512]{1,0:T(8,128)(2,1)} custom-call(bf16[256,512]{1,0:T(8,128)(2,1)} %refs_0_.1, bf16[256,512]{1,0:T(8,128)(2,1)} %refs_1_.1, bf16[256,256]{1,0:T(8,128)(2,1)} %refs_2_.1, bf16[32,256]{1,0:T(8,128)(2,1)} %bitcast.15, f32[1,512]{1,0:T(1,128)} %bitcast.16, f32[1,256]{1,0:T(1,128)} %bitcast.21, bf16[96,512]{1,0:T(8,128)(2,1)} %bitcast.12, ...), custom_call_target="tpu_custom_call" | custom-call | tf_op jit(solution)/shard_map/layer/pallas_call | solution.py:777
  109.5 1.7 %copy.28 = bf16[256,512]{1,0:T(8,128)(2,1)} copy(bf16[256,512]{1,0:T(8,128)(2,1)} %layer.1) | data formatting | bytes 524288

commit v3 on v2

--- a/solution.py
+++ b/solution.py
@@ -679,36 +679,38 @@
     start_down(max(last, 2))
     weights_here(2, 0)
     early = [*range(1, last), 0]
-    for k in early[:1] + early[-1:] + early[1:-1] if last > 1 else [0]:
-        if k > 1:
-            relay_far(k)
-            compute(k)
+    if last > 1:
+        unit(0, 1)
+    unit(0, 0)
+    if last > 0:
+        push_second(0)
+        relay(last, edge)
+    for k in range(2, last):
+        relay_far(k)
+        compute(k)
         unit(0, k)
-    push_second(0)
     if last > 0:
-        relay(last, edge)
+        push_second(0)
         weights_here(2, 1)
         for k in early:
             unit(1, k)
         push_second(0)
+        relay_far(last)
         for c in range(2, groups):
             pass_weights(2, c)
         push_third(3)
-        relay_far(last)
+        compute(last)
+        for c in range(2):
+            unit(c, last)
     for c in range(2, groups):
+        push_second(0)
+        if c == 2:
+            push_third(4)
         weights_here(2, c)
-        if c > 2:
-            unit(c, last)
-        for k in early:
+        for k in [last, *early[:-1]]:
             unit(c, k)
-        if c == 2:
-            compute(last)
-            for b in range(3):
-                unit(b, last)
-    if last in (1, 2):
-        compute(last)
-        for c in range(groups):
-            unit(c, last)
+    for c in range(2, groups):
+        unit(c, 0)
     push_second(0)
     push_third(0)
 

time: 111 us -> 109 us (0.982)
  Pallas kernels: 110 us -> 107 us
    pallas_call x1, Pallas kernels: 110 us -> 107 us  [whole_layer(): pl.pallas_call(functools.partial(layer_kernel, groups, turns, parts, stag...]
where the time goes in v3:
time: 109 us
  Pallas kernels  107 us (98%)
  local copies, waits for them, and re-layouts  1.67 us (2%)
    pallas_call x1, Pallas kernels, whole_layer(): pl.pallas_call(functools.partial(layer_kernel, groups, turns, parts, stag...  107 us

profile of v3, /device:TPU:1, one launch (start us, length us, event | category | flops | bytes accessed | tf_op | source)
XLA Modules:
  0.0 108.7 jit_solution(4427932447235212327)
XLA Ops:
  0.0 107.0 %layer.1 = bf16[256,512]{1,0:T(8,128)(2,1)} custom-call(bf16[256,512]{1,0:T(8,128)(2,1)} %refs_0_.1, bf16[256,512]{1,0:T(8,128)(2,1)} %refs_1_.1, bf16[256,256]{1,0:T(8,128)(2,1)} %refs_2_.1, bf16[32,256]{1,0:T(8,128)(2,1)} %bitcast.15, f32[1,512]{1,0:T(1,128)} %bitcast.16, f32[1,256]{1,0:T(1,128)} %bitcast.21, bf16[96,512]{1,0:T(8,128)(2,1)} %bitcast.12, ...), custom_call_target="tpu_custom_call" | custom-call | tf_op jit(solution)/shard_map/layer/pallas_call | solution.py:779
  107.0 1.7 %copy.28 = bf16[256,512]{1,0:T(8,128)(2,1)} copy(bf16[256,512]{1,0:T(8,128)(2,1)} %layer.1) | data formatting | bytes 524288
